TPU v7x, 32 devices: a whole 2x2x4 slice. The times are simulated.
32 devices in a mesh: sp: 4 (over y, x), tp: 8 (over z, core).
Axes of the slice: x: 2, y: 2, z: 4, core: 2. Of those that a mesh axis runs over, the one named last changes fastest.
Arguments:
- resid: bfloat16 [2048, 2048], P(('sp', 'tp')), may hold values from -6 to 6
- query_a: bfloat16 [2048, 16, 128], P('sp', 'tp'), may hold values from -16 to 16
- key_a: bfloat16 [2048, 16, 128], P('sp', 'tp'), may hold values from -16 to 16
- value_a: bfloat16 [2048, 16, 128], P('sp', 'tp'), may hold values from -6 to 6
- query_b: bfloat16 [2048, 16, 64], P('sp', 'tp'), may hold values from -16 to 16
- key_b: bfloat16 [2048, 16, 64], P('sp', 'tp'), may hold values from -16 to 16
- value_b: bfloat16 [2048, 16, 64], P('sp', 'tp'), may hold values from -6 to 6
- mix_a: float32 [16], P('tp'), may hold values from 0.3 to 0.8
- mix_b: float32 [16], P('tp'), may hold values from 0.3 to 0.8
- head_gain_a: float32 [128], replicated, may hold values from 0.1 to 1.9
- head_gain_b: float32 [64], replicated, may hold values from 0.1 to 1.9
- proj_a: bfloat16 [2048, 2048], P('tp'), may hold values from -0.109375 to 0.109375
- proj_b: bfloat16 [1024, 2048], P('tp'), may hold values from -0.109375 to 0.109375
- norm_gain: float32 [2048], replicated, may hold values from 0.1 to 1.9
- route_ids: int32 [2048, 2], P(('sp', 'tp')), may hold values from 0 to 3, all different within a row; in each aligned block of 64 rows (0 to 63, 64 to 127, ...) at most 48 rows name the same one
- route_weights: float32 [2048, 2], P(('sp', 'tp')), may hold values from 0.2 to 1
- expert_gate: bfloat16 [4, 2048, 6144], P('sp', None, 'tp'), may hold values from -0.125 to 0.125
- expert_up: bfloat16 [4, 2048, 6144], P('sp', None, 'tp'), may hold values from -0.125 to 0.125
- expert_down: bfloat16 [4, 6144, 2048], P('sp', 'tp'), may hold values from -0.078125 to 0.078125
Outputs:
- out: bfloat16 [2048, 2048], P(('sp', 'tp'))
Inputs may be any that keep to these rules, and one draw needn't show every extreme that they name: `route_ids`: each row names 2 different experts. Within the rows of one device (aligned blocks of 64 rows) no expert is named by more than 48 rows, and in every draw some device's block names some expert exactly 48 times.
All inputs are finite; a program needn't handle non-finite values.
Results may differ from a plain program's by a relative error of at most 0.02.
Values may be sent and summed in bfloat16 or wider, within the bound.
No kernel may reach another device: no remote copies, remote signals or barrier semaphores. Data moves between devices by JAX's collectives and lax.ppermute only.
A program may use at most 128 MiB of HBM per device.

v0:
```python
import math
import jax
import jax.numpy as jnp
from jax import lax
from jax.sharding import PartitionSpec as P

EPS = 1e-06
NEG = -1e30
HEAD_SCALE = 1.0 - (0.8 - 0.6 * math.exp(-0.3))
KEY_STEP = 512


def partner(value, axis, apart):
    return lax.ppermute(value, axis, [(i, i ^ 1 << apart) for i in range(lax.axis_size(axis))])


def rms_scaled(values, gain):
    return values * lax.rsqrt(jnp.mean(values * values, axis=-1, keepdims=True) + EPS) * gain


def slot_numbers(route_rows, experts, capacity):
    count, top_count = route_rows.shape
    flat = route_rows.reshape(count * top_count)
    onehot = (flat[:, None] == jnp.arange(experts, dtype=jnp.int32)[None, :]).astype(jnp.int32)
    ranks = jnp.sum((jnp.cumsum(onehot, axis=0) - onehot) * onehot, axis=1)
    return (flat * capacity + ranks).reshape(count, top_count)


def empty_map(count, heads, width):
    return (
        jnp.zeros((count, heads, width), jnp.float32),
        jnp.full((heads, count), NEG, jnp.float32),
        jnp.zeros((heads, count), jnp.float32),
    )


def empty_group(query, value):
    return (
        empty_map(query.shape[0], query.shape[1], value.shape[2]),
        empty_map(query.shape[0], query.shape[1], value.shape[2]),
    )


def map_update(state, query, keys, values, allowed, scale):
    weighted, maximum, sums = state
    scores = jnp.einsum("qhd,khd->hqk", query, keys, preferred_element_type=jnp.float32) * scale
    scores = jnp.where(allowed[None], scores, NEG)
    fresh = jnp.maximum(maximum, jnp.max(scores, axis=2))
    weights = jnp.where(allowed[None], jnp.exp(scores - fresh[:, :, None]), 0.0)
    factor = jnp.exp(maximum - fresh)
    sums = sums * factor + jnp.sum(weights, axis=2)
    added = jnp.einsum(
        "hqk,khv->qhv", weights.astype(jnp.bfloat16), values, preferred_element_type=jnp.float32
    )
    weighted = weighted * jnp.transpose(factor)[:, :, None] + added
    return (weighted, fresh, sums)


def group_update(states, query, keys, values, allowed):
    width = query.shape[2] // 2
    scale = 1.0 / math.sqrt(width)
    return tuple(
        (
            map_update(
                states[which],
                query[:, :, which * width : (which + 1) * width],
                keys[:, :, which * width : (which + 1) * width],
                values,
                allowed,
                scale,
            )
            for which in range(2)
        )
    )


def set_update(carry, queries, pieces):
    rows_a, rows_b, query_pos = queries
    piece_key_a, piece_value_a, piece_key_b, piece_value_b = pieces
    length = piece_key_a.shape[0]
    step = math.gcd(length, KEY_STEP)
    latest = query_pos[-1]

    def inner(index, states):
        first = index * step

        def compute(current):
            keys_a = lax.dynamic_slice_in_dim(piece_key_a, first, step, 0)
            values_a = lax.dynamic_slice_in_dim(piece_value_a, first, step, 0)
            keys_b = lax.dynamic_slice_in_dim(piece_key_b, first, step, 0)
            values_b = lax.dynamic_slice_in_dim(piece_value_b, first, step, 0)
            key_pos = first + jnp.arange(step, dtype=jnp.int32)
            allowed = key_pos[None, :] <= query_pos[:, None]
            return (
                group_update(current[0], rows_a, keys_a, values_a, allowed),
                group_update(current[1], rows_b, keys_b, values_b, allowed),
            )

        return lax.cond(first <= latest, compute, lambda current: current, states)

    return lax.fori_loop(0, length // step, inner, carry)


def finish_group(states, mix, gain):
    outputs = [state[0] / jnp.transpose(state[2])[:, :, None] for state in states]
    mixed = outputs[0] - mix[None, :, None] * outputs[1]
    normed = rms_scaled(mixed, gain) * HEAD_SCALE
    return normed.astype(jnp.bfloat16).reshape(mixed.shape[0], -1)


def per_device(
    resid,
    query_a,
    key_a,
    value_a,
    query_b,
    key_b,
    value_b,
    mix_a,
    mix_b,
    head_gain_a,
    head_gain_b,
    proj_a,
    proj_b,
    norm_gain,
    route_ids,
    route_weights,
    expert_gate,
    expert_up,
    expert_down,
):
    seq_rows = query_a.shape[0]
    sp_ways = lax.axis_size("sp")
    place = lax.axis_index("sp")
    positions = place * seq_rows + jnp.arange(seq_rows, dtype=jnp.int32)
    levels = sp_ways.bit_length() - 1
    half = seq_rows // 2
    moved = jnp.concatenate(
        [query_a[half:].reshape(half, -1), query_b[half:].reshape(half, -1)], axis=1
    )
    for bit in range(levels):
        moved = partner(moved, "sp", bit)
    split_at = query_a.shape[1] * query_a.shape[2]
    far_a = moved[:, :split_at].reshape(half, query_a.shape[1], query_a.shape[2])
    far_b = moved[:, split_at:].reshape(half, query_b.shape[1], query_b.shape[2])
    far_pos = (sp_ways - 1 - place) * seq_rows + half + jnp.arange(half, dtype=jnp.int32)
    query_sets = ((query_a[:half], query_b[:half], positions[:half]), (far_a, far_b, far_pos))

    def fold_keys(carry, pieces):
        return tuple(
            (set_update(states, queries, pieces) for states, queries in zip(carry, query_sets))
        )

    initial = tuple(
        (
            (empty_group(queries[0], value_a), empty_group(queries[1], value_b))
            for queries in query_sets
        )
    )
    results = fold_keys(
        initial,
        (
            lax.all_gather(key_a, "sp", axis=0, tiled=True),
            lax.all_gather(value_a, "sp", axis=0, tiled=True),
            lax.all_gather(key_b, "sp", axis=0, tiled=True),
            lax.all_gather(value_b, "sp", axis=0, tiled=True),
        ),
    )
    finished = [
        (finish_group(states[0], mix_a, head_gain_a), finish_group(states[1], mix_b, head_gain_b))
        for states in results
    ]
    returned = jnp.concatenate([finished[1][0], finished[1][1]], axis=1)
    for bit in range(levels):
        returned = partner(returned, "sp", bit)
    width_a = finished[0][0].shape[1]
    heads_out_a = jnp.concatenate([finished[0][0], returned[:, :width_a]], axis=0)
    heads_out_b = jnp.concatenate([finished[0][1], returned[:, width_a:]], axis=0)
    width = resid.shape[1]
    tok_rows = resid.shape[0]
    top_count = route_ids.shape[1]
    capacity = 3 * top_count * tok_rows // (2 * sp_ways)
    own_slots = slot_numbers(route_ids, sp_ways, capacity)
    term = jnp.dot(heads_out_a, proj_a, preferred_element_type=jnp.float32)
    term = term + jnp.dot(heads_out_b, proj_b, preferred_element_type=jnp.float32)
    mixed = resid.astype(jnp.float32) + lax.psum_scatter(
        lax.optimization_barrier(term.astype(jnp.bfloat16))
        .astype(jnp.float32)
        .astype(jnp.bfloat16),
        "tp",
        scatter_dimension=0,
        tiled=True,
    ).astype(jnp.float32)
    normed = rms_scaled(mixed, norm_gain).astype(jnp.bfloat16)
    lookup = jnp.arange(sp_ways * capacity, dtype=jnp.int32)[:, None]
    spread = jnp.zeros((sp_ways * capacity, tok_rows), jnp.float32)
    for which in range(top_count):
        spread = spread + (own_slots[:, which][None, :] == lookup).astype(jnp.float32)
    outgoing = jnp.dot(
        spread.astype(jnp.bfloat16), normed, preferred_element_type=jnp.float32
    ).astype(jnp.bfloat16)
    arrived = lax.all_to_all(
        outgoing.reshape(sp_ways, capacity, width), "sp", split_axis=0, concat_axis=0, tiled=True
    )
    piece = lax.all_gather(arrived.reshape(sp_ways * capacity, width), "tp", axis=0, tiled=True)
    gate = jnp.dot(piece, expert_gate[0], preferred_element_type=jnp.float32)
    upward = jnp.dot(piece, expert_up[0], preferred_element_type=jnp.float32)
    hidden = (jax.nn.silu(gate) * upward).astype(jnp.bfloat16)
    term = jnp.dot(hidden, expert_down[0], preferred_element_type=jnp.float32)
    summed = lax.psum_scatter(
        lax.optimization_barrier(term.astype(jnp.bfloat16))
        .astype(jnp.float32)
        .astype(jnp.bfloat16),
        "tp",
        scatter_dimension=0,
        tiled=True,
    )
    finished_rows = summed.reshape(sp_ways, capacity, width)
    back = lax.all_to_all(finished_rows, "sp", split_axis=0, concat_axis=0, tiled=True)
    picked = jnp.take(back.reshape(sp_ways * capacity, width), own_slots.reshape(-1), axis=0)
    picked = picked.reshape(tok_rows, top_count, width)
    output = mixed + jnp.sum(route_weights[:, :, None] * picked.astype(jnp.float32), axis=1)
    return output.astype(jnp.bfloat16)


def solution(mesh):
    placed = (
        P(("sp", "tp"), None),
        P("sp", "tp", None),
        P("sp", "tp", None),
        P("sp", "tp", None),
        P("sp", "tp", None),
        P("sp", "tp", None),
        P("sp", "tp", None),
        P("tp"),
        P("tp"),
        P(),
        P(),
        P("tp", None),
        P("tp", None),
        P(),
        P(("sp", "tp"), None),
        P(("sp", "tp"), None),
        P("sp", None, "tp"),
        P("sp", None, "tp"),
        P("sp", "tp", None),
    )
    return jax.shard_map(
        per_device, mesh=mesh, in_specs=placed, out_specs=P(("sp", "tp"), None), check_vma=False
    )
```

profile of v0, /device:TPU:0, one launch (start us, length us, event | category | flops | bytes accessed | tf_op | source)
XLA Modules:
  0.0 423.4 jit_solution(7599969802928675392)
XLA Ops:
  19.5 4.5 %collective-permute-done = bf16[256,384]{0,1:T(8,128)(2,1)} collective-permute-done((bf16[256,384]{0,1:T(8,128)(2,1)}, bf16[256,384]{0,1:T(8,128)(2,1)}, u32[]{:S(2)}, u32[]{:S(2)}) %collective-permute-start) | collective-permute-done | bytes 196640 | tf_op jit(solution)/shard_map/ppermute | solution.py:14
  25.3 16.1 %all_gather.17 = bf16[2048,2,64]{0,2,1:T(8,128)(2,1)} all-gather(bf16[512,2,64]{0,2,1:T(8,128)(2,1)} %param.32), channel_id=1, replica_groups=mesh['sp'=4,'tp'=8] {'sp'}, dimensions={0}, use_global_device_ids=true | all-gather | bytes 655360 | tf_op jit(solution)/shard_map/all_gather | solution.py:165
  41.4 10.7 %all_gather.18 = bf16[2048,2,64]{0,2,1:T(8,128)(2,1)} all-gather(bf16[512,2,64]{0,2,1:T(8,128)(2,1)} %param.33), channel_id=1, replica_groups=mesh['sp'=4,'tp'=8] {'sp'}, dimensions={0}, use_global_device_ids=true | all-gather | bytes 655360 | tf_op jit(solution)/shard_map/all_gather | solution.py:166
  53.4 17.1 %all-gather.6.cloned.1.call-done = bf16[2048,2,128]{0,2,1:T(8,128)(2,1)} async-done(((bf16[512,2,128]{0,2,1:T(8,128)(2,1)}), bf16[2048,2,128]{0,2,1:T(8,128)(2,1)}) %all-gather.6.cloned.1.call-update) | async-done | bytes 1048592 | tf_op jit(solution)/shard_map/all_gather | solution.py:164
  74.9 65.4 %while.72 = (s32[]{:T(128)}, f32[256,2,128]{0,2,1:T(8,128)S(1)}, f32[2,256]{1,0:T(2,128)S(1)}, f32[2,256]{1,0:T(2,128)}, f32[256,2,128]{0,2,1:T(8,128)}, /*index...) while((s32[]{:T(128)}, f32[256,2,128]{0,2,1:T(8,128)S(1)}, ...), condition=%wide.region_24.25_spmd.clone, body=%wide.region_13.24_spmd.clone.sunk | while | flops 311958272 | bytes 29590432 | solution.py:101
  75.5 15.7 %conditional.6 = ((f32[256,2,128]{0,2,1:T(8,128)S(1)}, f32[2,256]{1,0:T(2,128)S(1)}, f32[2,256]{1,0:T(2,128)}, f32[256,2,128]{0,2,1:T(8,128)}, f32[2,256]{1,0:T(...) conditional(s32[]{:T(128)} %convert_element_type.167, ...), branch_computations={%region_14.14_spmd, %region_15.23_spmd} | conditional | flops 311958272 | bytes 29588914 | solution.py:99
  91.8 15.8 %conditional.6 = ((f32[256,2,128]{0,2,1:T(8,128)S(1)}, f32[2,256]{1,0:T(2,128)S(1)}, f32[2,256]{1,0:T(2,128)}, f32[256,2,128]{0,2,1:T(8,128)}, f32[2,256]{1,0:T(...) conditional(s32[]{:T(128)} %convert_element_type.167, ...), branch_computations={%region_14.14_spmd, %region_15.23_spmd} | conditional | flops 311958272 | bytes 29588914 | solution.py:99
  108.2 15.7 %conditional.6 = ((f32[256,2,128]{0,2,1:T(8,128)S(1)}, f32[2,256]{1,0:T(2,128)S(1)}, f32[2,256]{1,0:T(2,128)}, f32[256,2,128]{0,2,1:T(8,128)}, f32[2,256]{1,0:T(...) conditional(s32[]{:T(128)} %convert_element_type.167, ...), branch_computations={%region_14.14_spmd, %region_15.23_spmd} | conditional | flops 311958272 | bytes 29588914 | solution.py:99
  124.5 15.7 %conditional.6 = ((f32[256,2,128]{0,2,1:T(8,128)S(1)}, f32[2,256]{1,0:T(2,128)S(1)}, f32[2,256]{1,0:T(2,128)}, f32[256,2,128]{0,2,1:T(8,128)}, f32[2,256]{1,0:T(...) conditional(s32[]{:T(128)} %convert_element_type.167, ...), branch_computations={%region_14.14_spmd, %region_15.23_spmd} | conditional | flops 311958272 | bytes 29588914 | solution.py:99
  145.4 19.4 %while.71 = (s32[]{:T(128)}, f32[256,2,128]{0,2,1:T(8,128)S(1)}, f32[2,256]{1,0:T(2,128)S(1)}, f32[2,256]{1,0:T(2,128)}, f32[256,2,128]{0,2,1:T(8,128)}, /*index...) while((s32[]{:T(128)}, f32[256,2,128]{0,2,1:T(8,128)S(1)}, ...), condition=%wide.region_11.12_spmd, body=%wide.region_0.11_spmd.sunk | while | flops 311958016 | bytes 29587348 | solution.py:101
  146.0 16.9 %conditional.5 = ((f32[256,2,128]{0,2,1:T(8,128)S(1)}, f32[2,256]{1,0:T(2,128)S(1)}, f32[2,256]{1,0:T(2,128)}, f32[256,2,128]{0,2,1:T(8,128)}, f32[2,256]{1,0:T(...) conditional(s32[]{:T(128)} %convert_element_type.166, ...), branch_computations={%region_1.0_spmd, %region_2.10_spmd} | conditional | flops 311958016 | bytes 29586862 | solution.py:99
  171.8 4.7 %collective-permute-done.2 = bf16[256,384]{0,1:T(8,128)(2,1)S(1)} collective-permute-done((bf16[256,384]{0,1:T(8,128)(2,1)S(1)}, bf16[256,384]{0,1:T(8,128)(2,1)S(1)}, u32[]{:S(2)}, u32[]{:S(2)}) %collective-permute-start.2) | collective-permute-done | bytes 196640 | tf_op jit(solution)/shard_map/ppermute | solution.py:14
  179.4 3.9 collective-permute-done.3
  187.2 36.5 %reduce-scatter.3.cloned.1.call-done = bf16[64,2048]{1,0:T(8,128)(2,1)} async-done(((bf16[512,2048]{1,0:T(8,128)(2,1)}), bf16[64,2048]{1,0:T(8,128)(2,1)}) %reduce-scatter.3.cloned.1.call-update) | async-done | bytes 262160 | tf_op jit(solution)/shard_map/reduce_scatter | solution.py:186
  226.3 12.3 %all_to_all.10 = bf16[4,48,2048]{2,1,0:T(8,128)(2,1)} all-to-all(bf16[4,48,2048]{2,1,0:T(8,128)(2,1)S(1)} %bitcast.127), channel_id=1, replica_groups=mesh['sp'=4,'tp'=8] {'sp'}, dimensions={0} | all-to-all | bytes 1572864 | tf_op jit(solution)/shard_map/all_to_all | solution.py:202
  238.8 63.9 %all-gather.8.cloned.1.call-done = bf16[1536,2048]{1,0:T(8,128)(2,1)} async-done(((bf16[192,2048]{1,0:T(8,128)(2,1)}), bf16[1536,2048]{1,0:T(8,128)(2,1)}) %all-gather.8.cloned.1.call-update) | async-done | bytes 6291472 | tf_op jit(solution)/shard_map/all_gather | solution.py:205
  302.7 8.2 %fusion.132 = f32[1536,768]{1,0:T(8,128)S(1)} fusion(bf16[1536,2048]{1,0:T(8,128)(2,1)} %all-gather.8.cloned.1.call-done, bf16[1,2048,768]{2,1,0:T(8,128)(2,1)} %param.43), kind=kOutput, calls=%fused_computation.172 | convolution fusion | flops 4831838208 | bytes 14155776 | tf_op jit(solution)/shard_map/dot_general | solution.py:206
  311.0 5.6 %multiply_convert_fusion = bf16[1536,768]{1,0:T(8,128)(2,1)S(1)} fusion(f32[1536,768]{1,0:T(8,128)S(1)} %fusion.132, bf16[1536,2048]{1,0:T(8,128)(2,1)S(1)} %copy-done.24, bf16[1,2048,768]{2,1,0:T(8,128)(2,1)S(1)} %copy-done.25), kind=kOutput, calls=%fused_computation.168 | convolution fusion | flops 4838916096 | bytes 16515072 | tf_op jit(solution)/shard_map/dot_general | solution.py:207
  316.6 7.1 %convolution_convert_fusion = bf16[1536,2048]{1,0:T(8,128)(2,1)} fusion(bf16[1536,768]{1,0:T(8,128)(2,1)S(1)} %multiply_convert_fusion, bf16[1,768,2048]{2,1,0:T(8,128)(2,1)S(1)} %copy-done), kind=kOutput, calls=%fused_computation.167 | convolution fusion | flops 4834983936 | bytes 11796480 | tf_op jit(solution)/shard_map/dot_general | solution.py:209
  323.7 68.5 %reduce-scatter.5.cloned.1.call-done = bf16[192,2048]{1,0:T(8,128)(2,1)} async-done(((bf16[1536,2048]{1,0:T(8,128)(2,1)}), bf16[192,2048]{1,0:T(8,128)(2,1)}) %reduce-scatter.5.cloned.1.call-update) | async-done | bytes 786448 | tf_op jit(solution)/shard_map/reduce_scatter | solution.py:210
  392.3 4.2 all-to-all-start.1
  396.9 8.8 %all-to-all-done.1 = bf16[4,48,2048]{2,1,0:T(8,128)(2,1)} async-done(((bf16[4,48,2048]{2,1,0:T(8,128)(2,1)}), bf16[4,48,2048]{2,1,0:T(8,128)(2,1)}, u32[]{:S(2)}, u32[]{:S(2)}) %all-to-all-start.1) | async-done | bytes 786464 | tf_op jit(solution)/shard_map/all_to_all | solution.py:219
  405.7 3.5 gather_fusion
  411.4 3.7 multiply_reduce_fusion
  (302 shorter events, 124.8 us)
Async XLA Ops:
  6.5 310.0 %copy-start = (bf16[1,768,2048]{2,1,0:T(8,128)(2,1)S(1)}, bf16[1,768,2048]{2,1,0:T(8,128)(2,1)}, u32[]{:S(2)}) copy-start(bf16[1,768,2048]{2,1,0:T(8,128)(2,1)} %param.45) | copy-start | bytes 9437188
  6.5 46.9 %all-gather.4.cloned.1.call-start = ((), (), s32[]{:S(2)}) async-start(), calls=%async_computation.4 | async-start | bytes 1310720 | tf_op jit(solution)/shard_map/all_gather | solution.py:163
  8.5 62.0 %all-gather.6.cloned.1.call-start = ((), (), s32[]{:S(2)}) async-start(), calls=%async_computation.5 | async-start | bytes 1310720 | tf_op jit(solution)/shard_map/all_gather | solution.py:164
  10.4 213.3 %reduce-scatter.3.cloned.1.call-start = ((), (), s32[]{:S(2)}) async-start(), calls=%async_computation.6 | async-start | bytes 2359296 | tf_op jit(solution)/shard_map/reduce_scatter | solution.py:186
  14.0 10.0 %collective-permute-start = (bf16[256,384]{0,1:T(8,128)(2,1)}, bf16[256,384]{0,1:T(8,128)(2,1)}, u32[]{:S(2)}, u32[]{:S(2)}) collective-permute-start(bf16[256,384]{0,1:T(8,128)(2,1)} %pad_maximum_fusion), channel_id=1, source_target_pairs={{0,8},{8,0},{16,24},{24,16},{1,9},{9,1},{17,25},{25,17},{2,10},{10... | collective-permute-start | bytes 589832 | tf_op jit(solution)/shard_map/ppermute | solution.py:14
  24.0 28.1 %collective-permute-start.1 = (bf16[256,384]{0,1:T(8,128)(2,1)}, bf16[256,384]{0,1:T(8,128)(2,1)S(1)}, u32[]{:S(2)}, u32[]{:S(2)}) collective-permute-start(bf16[256,384]{0,1:T(8,128)(2,1)} %collective-permute-done), channel_id=1, source_target_pairs={{0,16},{8,24},{16,0},{24,8},{1,17},{9,25},{17,1},{25,9},{2,18},{10... | collective-permute-start | bytes 589832 | tf_op jit(solution)/shard_map/ppermute | solution.py:14
  94.9 8.0 %copy-start.3 = (bf16[2048,2,128]{0,2,1:T(8,128)(2,1)S(1)}, bf16[2048,2,128]{0,2,1:T(8,128)(2,1)}, u32[]{:S(2)}) copy-start(bf16[2048,2,128]{0,2,1:T(8,128)(2,1)} %get-tuple-element.863) | copy-start | bytes 3145732 | tf_op jit(solution)/shard_map/while/body/eval_jaxpr/cond
  94.9 8.0 %copy-start.10 = (f32[256,2,128]{0,2,1:T(8,128)S(1)}, f32[256,2,128]{0,2,1:T(8,128)}, u32[]{:S(2)}) copy-start(f32[256,2,128]{0,2,1:T(8,128)} %get-tuple-element.865) | copy-start | bytes 786436 | tf_op jit(solution)/shard_map/while/body/eval_jaxpr/cond
  94.9 8.0 %copy-start.19 = (f32[256,2]{0,1:T(2,128)S(1)}, f32[256,2]{0,1:T(2,128)}, u32[]{:S(2)}) copy-start(f32[256,2]{0,1:T(2,128)} %get-tuple-element.1107) | copy-start | bytes 6148 | tf_op jit(solution)/shard_map/while/body/eval_jaxpr/cond
  111.2 8.0 %copy-start.3 = (bf16[2048,2,128]{0,2,1:T(8,128)(2,1)S(1)}, bf16[2048,2,128]{0,2,1:T(8,128)(2,1)}, u32[]{:S(2)}) copy-start(bf16[2048,2,128]{0,2,1:T(8,128)(2,1)} %get-tuple-element.863) | copy-start | bytes 3145732 | tf_op jit(solution)/shard_map/while/body/eval_jaxpr/cond
  111.2 8.0 %copy-start.10 = (f32[256,2,128]{0,2,1:T(8,128)S(1)}, f32[256,2,128]{0,2,1:T(8,128)}, u32[]{:S(2)}) copy-start(f32[256,2,128]{0,2,1:T(8,128)} %get-tuple-element.865) | copy-start | bytes 786436 | tf_op jit(solution)/shard_map/while/body/eval_jaxpr/cond
  111.2 8.0 %copy-start.19 = (f32[256,2]{0,1:T(2,128)S(1)}, f32[256,2]{0,1:T(2,128)}, u32[]{:S(2)}) copy-start(f32[256,2]{0,1:T(2,128)} %get-tuple-element.1107) | copy-start | bytes 6148 | tf_op jit(solution)/shard_map/while/body/eval_jaxpr/cond
  164.7 18.6 %copy-start.14 = (bf16[128,2048]{1,0:T(8,128)(2,1)S(1)}, bf16[128,2048]{1,0:T(8,128)(2,1)}, u32[]{:S(2)}) copy-start(bf16[128,2048]{1,0:T(8,128)(2,1)} %param.39) | copy-start | bytes 1572868
  166.1 18.0 %copy-start.13 = (bf16[256,2048]{1,0:T(8,128)(2,1)S(1)}, bf16[256,2048]{1,0:T(8,128)(2,1)}, u32[]{:S(2)}) copy-start(bf16[256,2048]{1,0:T(8,128)(2,1)} %param.38) | copy-start | bytes 3145732
  169.0 7.5 %collective-permute-start.2 = (bf16[256,384]{0,1:T(8,128)(2,1)S(1)}, bf16[256,384]{0,1:T(8,128)(2,1)S(1)}, u32[]{:S(2)}, u32[]{:S(2)}) collective-permute-start(bf16[256,384]{0,1:T(8,128)(2,1)S(1)} %pad_maximum_fusion.1), channel_id=1, source_target_pairs={{0,8},{8,0},{16,24},{24,16},{1,9},{9,1},{17,25},{25,17},{2,10},{10... | collective-permute-start | bytes 589832 | tf_op jit(solution)/shard_map/ppermute | solution.py:14
  176.5 6.9 %collective-permute-start.3 = (bf16[256,384]{0,1:T(8,128)(2,1)S(1)}, bf16[256,384]{0,1:T(8,128)(2,1)S(1)}, u32[]{:S(2)}, u32[]{:S(2)}) collective-permute-start(bf16[256,384]{0,1:T(8,128)(2,1)S(1)} %collective-permute-done.2), channel_id=1, source_target_pairs={{0,16},{8,24},{16,0},{24,8},{1,17},{9,25},{17,1},{25,9},{2,18},{10... | collective-permute-start | bytes 589832 | tf_op jit(solution)/shard_map/ppermute | solution.py:14
  184.1 39.6 %copy-start.12 = (bf16[64,2048]{1,0:T(8,128)(2,1)S(1)}, bf16[64,2048]{1,0:T(8,128)(2,1)}, u32[]{:S(2)}) copy-start(bf16[64,2048]{1,0:T(8,128)(2,1)} %param.27) | copy-start | bytes 786436
  184.1 40.8 %copy-start.22 = (f32[2048]{0:T(1024)S(1)}, f32[2048]{0:T(1024)}, u32[]{:S(2)}) copy-start(f32[2048]{0:T(1024)} %param.40) | copy-start | bytes 24580
  186.3 116.5 %all-gather.8.cloned.1.call-start = ((), (), s32[]{:S(2)}) async-start(), calls=%async_computation.7 | async-start | bytes 7077888 | tf_op jit(solution)/shard_map/all_gather | solution.py:205
  238.6 153.7 %reduce-scatter.5.cloned.1.call-start = ((), (), s32[]{:S(2)}) async-start(), calls=%async_computation.8 | async-start | bytes 7077888 | tf_op jit(solution)/shard_map/reduce_scatter | solution.py:210
  302.7 8.2 %copy-start.24 = (bf16[1536,2048]{1,0:T(8,128)(2,1)S(1)}, bf16[1536,2048]{1,0:T(8,128)(2,1)}, u32[]{:S(2)}) copy-start(bf16[1536,2048]{1,0:T(8,128)(2,1)} %all-gather.8.cloned.1.call-done) | copy-start | bytes 18874372
  302.7 8.2 %copy-start.25 = (bf16[1,2048,768]{2,1,0:T(8,128)(2,1)S(1)}, bf16[1,2048,768]{2,1,0:T(8,128)(2,1)}, u32[]{:S(2)}) copy-start(bf16[1,2048,768]{2,1,0:T(8,128)(2,1)} %param.44) | copy-start | bytes 9437188
  323.7 73.1 %copy-start.23 = (f32[64,2]{0,1:T(2,128)S(1)}, f32[64,2]{0,1:T(2,128)}, u32[]{:S(2)}) copy-start(f32[64,2]{0,1:T(2,128)} %param.42) | copy-start | bytes 1540
  392.3 13.5 %all-to-all-start.1 = ((bf16[4,48,2048]{2,1,0:T(8,128)(2,1)}), bf16[4,48,2048]{2,1,0:T(8,128)(2,1)}, u32[]{:S(2)}, u32[]{:S(2)}) async-start(bf16[4,48,2048]{2,1,0:T(8,128)(2,1)} %bitcast.128), calls=%async_computation.3 | async-start | bytes 1572864 | tf_op jit(solution)/shard_map/all_to_all | solution.py:219
  (36 other events, 182.1 us)
Sparse Core Ops, SparseCore 0:
  9.2 32.6 all-gather.3
  43.7 26.7 all-gather.5
  186.4 37.3 reduce-scatter.2
  238.7 63.9 all-gather.7
  323.8 68.3 reduce-scatter.4
where the time goes:
time: 425 us; the launch traced here: 423 us
  waiting for transfers between devices  208 us (49%)
  matrix products  78.7 us (19%)
  blocking collectives  39.1 us (9%)
  other arithmetic  36.5 us (9%)
  local copies, waits for them, and re-layouts  27.2 us (6%)
  starting transfers between devices  14.5 us (3%)
  between operations  13.5 us (3%)
  loops' own time  5.82 us (1%)
    reduce_scatter x2, waiting for transfers between devices, per_device(): lax.psum_scatter(lax.optimization_barrier(term.astype(jnp.bfloat16)).asty...  105 us
    all_gather x1, waiting for transfers between devices, per_device(): lax.all_gather(arrived.reshape(sp_ways * capacity, width), 'tp', axis=0,...  63.9 us
    dot_general x20, matrix products, map_update(): jnp.einsum('qhd,khd->hqk', query, keys, preferred_element_type=jnp.float32)  30.7 us
    dot_general x20, matrix products, map_update(): jnp.einsum('hqk,khv->qhv', weights.astype(jnp.bfloat16), values, preferre...  22.8 us
    all_gather x1, waiting for transfers between devices, per_device(): lax.all_gather(value_a, 'sp', axis=0, tiled=True)  17.1 us
    all_gather x1, blocking collectives, per_device(): lax.all_gather(key_b, 'sp', axis=0, tiled=True)  16.1 us
    ppermute x4, waiting for transfers between devices, partner(): lax.ppermute(value, axis, [(i, i ^ 1 << apart) for i in range(lax.axis_si...  13.2 us
    add x10, other arithmetic, map_update(): sums = sums * factor + jnp.sum(weights, axis=2)  12.9 us
  transfers between devices with their start and end apart: 10, of which 8 were waited for; matrix products, arithmetic and copies ran while one was open for 2% of the time, Pallas kernels for 0%

commit v1 on v0

--- a/solution.py
+++ b/solution.py
@@ -202,7 +202,15 @@
     arrived = lax.all_to_all(
         outgoing.reshape(sp_ways, capacity, width), "sp", split_axis=0, concat_axis=0, tiled=True
     )
-    piece = lax.all_gather(arrived.reshape(sp_ways * capacity, width), "tp", axis=0, tiled=True)
+    piece = jnp.concatenate(
+        lax.all_to_all(
+            jnp.stack([arrived.reshape(sp_ways * capacity, width)] * lax.axis_size("tp")),
+            "tp",
+            0,
+            0,
+        ),
+        axis=0,
+    )
     gate = jnp.dot(piece, expert_gate[0], preferred_element_type=jnp.float32)
     upward = jnp.dot(piece, expert_up[0], preferred_element_type=jnp.float32)
     hidden = (jax.nn.silu(gate) * upward).astype(jnp.bfloat16)

time: 425 us -> 502 us (1.18)
  blocking collectives: 39.1 us -> 182 us
  waiting for transfers between devices: 208 us -> 143 us
    all_to_all x0 -> x1, blocking collectives: none -> 143 us  [per_device(): lax.all_to_all(jnp.stack([arrived.reshape(sp_ways * capacity, width)] * l...]
    all_gather x1 -> x0, waiting for transfers between devices: 63.9 us -> none  [per_device(): lax.all_gather(arrived.reshape(sp_ways * capacity, width), 'tp', axis=0,...]
  transfers between devices with their start and end apart: 10 -> 9, of which waited for: 8 -> 7; matrix products, arithmetic and copies ran while one was open for 2% -> 2% of each run, Pallas kernels for 0% -> 0%
where the time goes in v1:
time: 502 us; the launch traced here: 500 us
  blocking collectives  182 us (36%)
  waiting for transfers between devices  143 us (28%)
  matrix products  76 us (15%)
  other arithmetic  36.5 us (7%)
  local copies, waits for them, and re-layouts  28.2 us (6%)
  starting transfers between devices  14.6 us (3%)
  between operations  13.5 us (3%)
  loops' own time  6.34 us (1%)
    all_to_all x1, blocking collectives, per_device(): lax.all_to_all(jnp.stack([arrived.reshape(sp_ways * capacity, width)] * l...  143 us
    reduce_scatter x2, waiting for transfers between devices, per_device(): lax.psum_scatter(lax.optimization_barrier(term.astype(jnp.bfloat16)).asty...  104 us
    dot_general x20, matrix products, map_update(): jnp.einsum('qhd,khd->hqk', query, keys, preferred_element_type=jnp.float32)  30.9 us
    dot_general x20, matrix products, map_update(): jnp.einsum('hqk,khv->qhv', weights.astype(jnp.bfloat16), values, preferre...  23 us
    all_gather x1, waiting for transfers between devices, per_device(): lax.all_gather(value_a, 'sp', axis=0, tiled=True)  17 us
    all_gather x1, blocking collectives, per_device(): lax.all_gather(key_b, 'sp', axis=0, tiled=True)  16.2 us
    ppermute x4, waiting for transfers between devices, partner(): lax.ppermute(value, axis, [(i, i ^ 1 << apart) for i in range(lax.axis_si...  13.1 us
    add x10, other arithmetic, map_update(): sums = sums * factor + jnp.sum(weights, axis=2)  12.9 us
  transfers between devices with their start and end apart: 9, of which 7 were waited for; matrix products, arithmetic and copies ran while one was open for 2% of the time, Pallas kernels for 0%

profile of v1, /device:TPU:0, one launch (start us, length us, event | category | flops | bytes accessed | tf_op | source)
XLA Modules:
  0.0 500.0 jit_solution(13080105872777136164)
XLA Ops:
  19.5 4.5 collective-permute-done
  25.3 16.2 %all_gather.14 = bf16[2048,2,64]{0,2,1:T(8,128)(2,1)} all-gather(bf16[512,2,64]{0,2,1:T(8,128)(2,1)} %param.32), channel_id=1, replica_groups=mesh['sp'=4,'tp'=8] {'sp'}, dimensions={0}, use_global_device_ids=true | all-gather | bytes 655360 | tf_op jit(solution)/shard_map/all_gather | solution.py:165
  41.4 10.7 %all_gather.15 = bf16[2048,2,64]{0,2,1:T(8,128)(2,1)} all-gather(bf16[512,2,64]{0,2,1:T(8,128)(2,1)} %param.33), channel_id=1, replica_groups=mesh['sp'=4,'tp'=8] {'sp'}, dimensions={0}, use_global_device_ids=true | all-gather | bytes 655360 | tf_op jit(solution)/shard_map/all_gather | solution.py:166
  53.4 17.0 %all-gather.5.cloned.1.call-done = bf16[2048,2,128]{0,2,1:T(8,128)(2,1)} async-done(((bf16[512,2,128]{0,2,1:T(8,128)(2,1)}), bf16[2048,2,128]{0,2,1:T(8,128)(2,1)}) %all-gather.5.cloned.1.call-update) | async-done | bytes 1048592 | tf_op jit(solution)/shard_map/all_gather | solution.py:164
  74.9 65.9 %while.72 = (s32[]{:T(128)}, f32[256,2,128]{0,2,1:T(8,128)S(1)}, f32[2,256]{1,0:T(2,128)S(1)}, f32[2,256]{1,0:T(2,128)}, f32[256,2,128]{0,2,1:T(8,128)}, /*index...) while((s32[]{:T(128)}, f32[256,2,128]{0,2,1:T(8,128)S(1)}, ...), condition=%wide.region_24.25_spmd.clone, body=%wide.region_13.24_spmd.clone.sunk | while | flops 311958272 | bytes 29590432 | solution.py:101
  75.6 15.8 %conditional.6 = ((f32[256,2,128]{0,2,1:T(8,128)S(1)}, f32[2,256]{1,0:T(2,128)S(1)}, f32[2,256]{1,0:T(2,128)}, f32[256,2,128]{0,2,1:T(8,128)}, f32[2,256]{1,0:T(...) conditional(s32[]{:T(128)} %convert_element_type.167, ...), branch_computations={%region_14.14_spmd, %region_15.23_spmd} | conditional | flops 311958272 | bytes 29588914 | solution.py:99
  92.0 15.8 %conditional.6 = ((f32[256,2,128]{0,2,1:T(8,128)S(1)}, f32[2,256]{1,0:T(2,128)S(1)}, f32[2,256]{1,0:T(2,128)}, f32[256,2,128]{0,2,1:T(8,128)}, f32[2,256]{1,0:T(...) conditional(s32[]{:T(128)} %convert_element_type.167, ...), branch_computations={%region_14.14_spmd, %region_15.23_spmd} | conditional | flops 311958272 | bytes 29588914 | solution.py:99
  108.5 15.8 %conditional.6 = ((f32[256,2,128]{0,2,1:T(8,128)S(1)}, f32[2,256]{1,0:T(2,128)S(1)}, f32[2,256]{1,0:T(2,128)}, f32[256,2,128]{0,2,1:T(8,128)}, f32[2,256]{1,0:T(...) conditional(s32[]{:T(128)} %convert_element_type.167, ...), branch_computations={%region_14.14_spmd, %region_15.23_spmd} | conditional | flops 311958272 | bytes 29588914 | solution.py:99
  125.0 15.8 %conditional.6 = ((f32[256,2,128]{0,2,1:T(8,128)S(1)}, f32[2,256]{1,0:T(2,128)S(1)}, f32[2,256]{1,0:T(2,128)}, f32[256,2,128]{0,2,1:T(8,128)}, f32[2,256]{1,0:T(...) conditional(s32[]{:T(128)} %convert_element_type.167, ...), branch_computations={%region_14.14_spmd, %region_15.23_spmd} | conditional | flops 311958272 | bytes 29588914 | solution.py:99
  145.9 19.7 %while.71 = (s32[]{:T(128)}, f32[256,2,128]{0,2,1:T(8,128)S(1)}, f32[2,256]{1,0:T(2,128)S(1)}, f32[2,256]{1,0:T(2,128)}, f32[256,2,128]{0,2,1:T(8,128)}, /*index...) while((s32[]{:T(128)}, f32[256,2,128]{0,2,1:T(8,128)S(1)}, ...), condition=%wide.region_11.12_spmd, body=%wide.region_0.11_spmd.sunk | while | flops 311958016 | bytes 29587348 | solution.py:101
  146.6 17.0 %conditional.5 = ((f32[256,2,128]{0,2,1:T(8,128)S(1)}, f32[2,256]{1,0:T(2,128)S(1)}, f32[2,256]{1,0:T(2,128)}, f32[256,2,128]{0,2,1:T(8,128)}, f32[2,256]{1,0:T(...) conditional(s32[]{:T(128)} %convert_element_type.166, ...), branch_computations={%region_1.0_spmd, %region_2.10_spmd} | conditional | flops 311958016 | bytes 29586862 | solution.py:99
  172.7 4.7 collective-permute-done.2
  180.5 3.9 collective-permute-done.3
  188.3 36.7 %reduce-scatter.3.cloned.1.call-done = bf16[64,2048]{1,0:T(8,128)(2,1)} async-done(((bf16[512,2048]{1,0:T(8,128)(2,1)}), bf16[64,2048]{1,0:T(8,128)(2,1)}) %reduce-scatter.3.cloned.1.call-update) | async-done | bytes 262160 | tf_op jit(solution)/shard_map/reduce_scatter | solution.py:186
  227.6 12.0 %all_to_all.15 = bf16[4,48,2048]{2,1,0:T(8,128)(2,1)S(1)} all-to-all(bf16[4,48,2048]{2,1,0:T(8,128)(2,1)S(1)} %bitcast.130), channel_id=1, replica_groups=mesh['sp'=4,'tp'=8] {'sp'}, dimensions={0} | all-to-all | bytes 1572864 | tf_op jit(solution)/shard_map/all_to_all | solution.py:202
  240.3 143.4 %all_to_all.16 = bf16[8,192,2048]{2,1,0:T(8,128)(2,1)S(1)} all-to-all(bf16[8,192,2048]{2,1,0:T(8,128)(2,1)S(1)} %stack.3), channel_id=1, replica_groups=mesh['sp'=4,'tp'=8] {'tp'}, dimensions={0} | all-to-all | bytes 12582912 | tf_op jit(solution)/shard_map/all_to_all | solution.py:206
  383.7 5.2 %fusion.132 = f32[1536,768]{1,0:T(8,128)S(1)} fusion(bf16[1536,2048]{1,0:T(8,128)(2,1)S(1)} %bitcast.127, bf16[1,2048,768]{2,1,0:T(8,128)(2,1)S(1)} %copy-done.24), kind=kOutput, calls=%fused_computation.172 | convolution fusion | flops 4831838208 | bytes 14155776 | tf_op jit(solution)/shard_map/dot_general | solution.py:214
  388.9 5.6 %multiply_convert_fusion = bf16[1536,768]{1,0:T(8,128)(2,1)S(1)} fusion(f32[1536,768]{1,0:T(8,128)S(1)} %fusion.132, bf16[1536,2048]{1,0:T(8,128)(2,1)S(1)} %bitcast.128, bf16[1,2048,768]{2,1,0:T(8,128)(2,1)S(1)} %copy-done.25), kind=kOutput, calls=%fused_computation.168 | convolution fusion | flops 4838916096 | bytes 16515072 | tf_op jit(solution)/shard_map/dot_general | solution.py:215
  394.6 7.1 %convolution_convert_fusion = bf16[1536,2048]{1,0:T(8,128)(2,1)} fusion(bf16[1536,768]{1,0:T(8,128)(2,1)S(1)} %multiply_convert_fusion, bf16[1,768,2048]{2,1,0:T(8,128)(2,1)S(1)} %copy-done), kind=kOutput, calls=%fused_computation.167 | convolution fusion | flops 4834983936 | bytes 11796480 | tf_op jit(solution)/shard_map/dot_general | solution.py:217
  401.7 67.3 %reduce-scatter.5.cloned.1.call-done = bf16[192,2048]{1,0:T(8,128)(2,1)} async-done(((bf16[1536,2048]{1,0:T(8,128)(2,1)}), bf16[192,2048]{1,0:T(8,128)(2,1)}) %reduce-scatter.5.cloned.1.call-update) | async-done | bytes 786448 | tf_op jit(solution)/shard_map/reduce_scatter | solution.py:218
  469.0 4.4 all-to-all-start.2
  473.9 8.6 %all-to-all-done.2 = bf16[4,48,2048]{2,1,0:T(8,128)(2,1)} async-done(((bf16[4,48,2048]{2,1,0:T(8,128)(2,1)}), bf16[4,48,2048]{2,1,0:T(8,128)(2,1)}, u32[]{:S(2)}, u32[]{:S(2)}) %all-to-all-start.2) | async-done | bytes 786464 | tf_op jit(solution)/shard_map/all_to_all | solution.py:227
  482.4 3.5 gather_fusion
  488.1 3.7 multiply_reduce_fusion
  (301 shorter events, 125.9 us)
Async XLA Ops:
  6.5 388.0 %copy-start = (bf16[1,768,2048]{2,1,0:T(8,128)(2,1)S(1)}, bf16[1,768,2048]{2,1,0:T(8,128)(2,1)}, u32[]{:S(2)}) copy-start(bf16[1,768,2048]{2,1,0:T(8,128)(2,1)} %param.45) | copy-start | bytes 9437188
  6.5 46.9 %all-gather.3.cloned.1.call-start = ((), (), s32[]{:S(2)}) async-start(), calls=%async_computation.5 | async-start | bytes 1310720 | tf_op jit(solution)/shard_map/all_gather | solution.py:163
  8.5 61.9 %all-gather.5.cloned.1.call-start = ((), (), s32[]{:S(2)}) async-start(), calls=%async_computation.6 | async-start | bytes 1310720 | tf_op jit(solution)/shard_map/all_gather | solution.py:164
  10.4 214.6 %reduce-scatter.3.cloned.1.call-start = ((), (), s32[]{:S(2)}) async-start(), calls=%async_computation.7 | async-start | bytes 2359296 | tf_op jit(solution)/shard_map/reduce_scatter | solution.py:186
  13.9 10.0 %collective-permute-start = (bf16[256,384]{0,1:T(8,128)(2,1)}, bf16[256,384]{0,1:T(8,128)(2,1)}, u32[]{:S(2)}, u32[]{:S(2)}) collective-permute-start(bf16[256,384]{0,1:T(8,128)(2,1)} %pad_maximum_fusion), channel_id=1, source_target_pairs={{0,8},{8,0},{16,24},{24,16},{1,9},{9,1},{17,25},{25,17},{2,10},{10... | collective-permute-start | bytes 589832 | tf_op jit(solution)/shard_map/ppermute | solution.py:14
  24.0 28.1 %collective-permute-start.1 = (bf16[256,384]{0,1:T(8,128)(2,1)}, bf16[256,384]{0,1:T(8,128)(2,1)S(1)}, u32[]{:S(2)}, u32[]{:S(2)}) collective-permute-start(bf16[256,384]{0,1:T(8,128)(2,1)} %collective-permute-done), channel_id=1, source_target_pairs={{0,16},{8,24},{16,0},{24,8},{1,17},{9,25},{17,1},{25,9},{2,18},{10... | collective-permute-start | bytes 589832 | tf_op jit(solution)/shard_map/ppermute | solution.py:14
  78.6 8.0 %copy-start.10 = (f32[256,2,128]{0,2,1:T(8,128)S(1)}, f32[256,2,128]{0,2,1:T(8,128)}, u32[]{:S(2)}) copy-start(f32[256,2,128]{0,2,1:T(8,128)} %get-tuple-element.865) | copy-start | bytes 786436 | tf_op jit(solution)/shard_map/while/body/eval_jaxpr/cond
  95.1 8.0 %copy-start.3 = (bf16[2048,2,128]{0,2,1:T(8,128)(2,1)S(1)}, bf16[2048,2,128]{0,2,1:T(8,128)(2,1)}, u32[]{:S(2)}) copy-start(bf16[2048,2,128]{0,2,1:T(8,128)(2,1)} %get-tuple-element.863) | copy-start | bytes 3145732 | tf_op jit(solution)/shard_map/while/body/eval_jaxpr/cond
  95.1 8.0 %copy-start.10 = (f32[256,2,128]{0,2,1:T(8,128)S(1)}, f32[256,2,128]{0,2,1:T(8,128)}, u32[]{:S(2)}) copy-start(f32[256,2,128]{0,2,1:T(8,128)} %get-tuple-element.865) | copy-start | bytes 786436 | tf_op jit(solution)/shard_map/while/body/eval_jaxpr/cond
  111.6 8.0 %copy-start.3 = (bf16[2048,2,128]{0,2,1:T(8,128)(2,1)S(1)}, bf16[2048,2,128]{0,2,1:T(8,128)(2,1)}, u32[]{:S(2)}) copy-start(bf16[2048,2,128]{0,2,1:T(8,128)(2,1)} %get-tuple-element.863) | copy-start | bytes 3145732 | tf_op jit(solution)/shard_map/while/body/eval_jaxpr/cond
  111.6 8.0 %copy-start.10 = (f32[256,2,128]{0,2,1:T(8,128)S(1)}, f32[256,2,128]{0,2,1:T(8,128)}, u32[]{:S(2)}) copy-start(f32[256,2,128]{0,2,1:T(8,128)} %get-tuple-element.865) | copy-start | bytes 786436 | tf_op jit(solution)/shard_map/while/body/eval_jaxpr/cond
  128.0 8.0 %copy-start.3 = (bf16[2048,2,128]{0,2,1:T(8,128)(2,1)S(1)}, bf16[2048,2,128]{0,2,1:T(8,128)(2,1)}, u32[]{:S(2)}) copy-start(bf16[2048,2,128]{0,2,1:T(8,128)(2,1)} %get-tuple-element.863) | copy-start | bytes 3145732 | tf_op jit(solution)/shard_map/while/body/eval_jaxpr/cond
  128.1 8.0 %copy-start.10 = (f32[256,2,128]{0,2,1:T(8,128)S(1)}, f32[256,2,128]{0,2,1:T(8,128)}, u32[]{:S(2)}) copy-start(f32[256,2,128]{0,2,1:T(8,128)} %get-tuple-element.865) | copy-start | bytes 786436 | tf_op jit(solution)/shard_map/while/body/eval_jaxpr/cond
  150.9 8.0 %copy-start.7 = (f32[256,2,128]{0,2,1:T(8,128)S(1)}, f32[256,2,128]{0,2,1:T(8,128)}, u32[]{:S(2)}) copy-start(f32[256,2,128]{0,2,1:T(8,128)} %get-tuple-element.811) | copy-start | bytes 786436 | tf_op jit(solution)/shard_map/while/body/eval_jaxpr/cond
  165.6 18.8 %copy-start.14 = (bf16[128,2048]{1,0:T(8,128)(2,1)S(1)}, bf16[128,2048]{1,0:T(8,128)(2,1)}, u32[]{:S(2)}) copy-start(bf16[128,2048]{1,0:T(8,128)(2,1)} %param.39) | copy-start | bytes 1572868
  167.0 18.2 %copy-start.13 = (bf16[256,2048]{1,0:T(8,128)(2,1)S(1)}, bf16[256,2048]{1,0:T(8,128)(2,1)}, u32[]{:S(2)}) copy-start(bf16[256,2048]{1,0:T(8,128)(2,1)} %param.38) | copy-start | bytes 3145732
  169.9 7.5 %collective-permute-start.2 = (bf16[256,384]{0,1:T(8,128)(2,1)S(1)}, bf16[256,384]{0,1:T(8,128)(2,1)S(1)}, u32[]{:S(2)}, u32[]{:S(2)}) collective-permute-start(bf16[256,384]{0,1:T(8,128)(2,1)S(1)} %pad_maximum_fusion.1), channel_id=1, source_target_pairs={{0,8},{8,0},{16,24},{24,16},{1,9},{9,1},{17,25},{25,17},{2,10},{10... | collective-permute-start | bytes 589832 | tf_op jit(solution)/shard_map/ppermute | solution.py:14
  177.4 7.0 %collective-permute-start.3 = (bf16[256,384]{0,1:T(8,128)(2,1)S(1)}, bf16[256,384]{0,1:T(8,128)(2,1)S(1)}, u32[]{:S(2)}, u32[]{:S(2)}) collective-permute-start(bf16[256,384]{0,1:T(8,128)(2,1)S(1)} %collective-permute-done.2), channel_id=1, source_target_pairs={{0,16},{8,24},{16,0},{24,8},{1,17},{9,25},{17,1},{25,9},{2,18},{10... | collective-permute-start | bytes 589832 | tf_op jit(solution)/shard_map/ppermute | solution.py:14
  185.2 39.9 %copy-start.12 = (bf16[64,2048]{1,0:T(8,128)(2,1)S(1)}, bf16[64,2048]{1,0:T(8,128)(2,1)}, u32[]{:S(2)}) copy-start(bf16[64,2048]{1,0:T(8,128)(2,1)} %param.27) | copy-start | bytes 786436
  185.2 41.0 %copy-start.22 = (f32[2048]{0:T(1024)S(1)}, f32[2048]{0:T(1024)}, u32[]{:S(2)}) copy-start(f32[2048]{0:T(1024)} %param.40) | copy-start | bytes 24580
  187.3 281.7 %reduce-scatter.5.cloned.1.call-start = ((), (), s32[]{:S(2)}) async-start(), calls=%async_computation.8 | async-start | bytes 7077888 | tf_op jit(solution)/shard_map/reduce_scatter | solution.py:218
  240.3 143.4 %copy-start.24 = (bf16[1,2048,768]{2,1,0:T(8,128)(2,1)S(1)}, bf16[1,2048,768]{2,1,0:T(8,128)(2,1)}, u32[]{:S(2)}) copy-start(bf16[1,2048,768]{2,1,0:T(8,128)(2,1)} %param.43) | copy-start | bytes 9437188
  401.6 72.1 %copy-start.23 = (f32[64,2]{0,1:T(2,128)S(1)}, f32[64,2]{0,1:T(2,128)}, u32[]{:S(2)}) copy-start(f32[64,2]{0,1:T(2,128)} %param.42) | copy-start | bytes 1540
  469.0 13.5 %all-to-all-start.2 = ((bf16[4,48,2048]{2,1,0:T(8,128)(2,1)}), bf16[4,48,2048]{2,1,0:T(8,128)(2,1)}, u32[]{:S(2)}, u32[]{:S(2)}) async-start(bf16[4,48,2048]{2,1,0:T(8,128)(2,1)} %bitcast.131), calls=%async_computation.4 | async-start | bytes 1572864 | tf_op jit(solution)/shard_map/all_to_all | solution.py:227
  (35 other events, 171.8 us)
Sparse Core Ops, SparseCore 0:
  9.2 32.6 all-gather.2
  43.7 26.7 all-gather.4
  187.4 37.5 reduce-scatter.2
  401.8 67.1 reduce-scatter.4
